TPU v7x, 128 devices: a whole 4x4x4 slice. The times are simulated.
128 devices in a mesh: ep: 16 (over z, x), tp: 8 (over y, core).
Axes of the slice: x: 4, y: 4, z: 4, core: 2. Of those that a mesh axis runs over, the one named last changes fastest.
Arguments:
- tokens: bfloat16 [16384, 2048], P(('ep', 'tp')), may hold values from -6 to 6
- expert_ids: int32 [16384, 4], P('ep'), may hold values from 0 to 15, all different within a row; in each aligned block of 128 rows (0 to 127, 128 to 255, ...) at most 64 rows name the same one
- gate_values: float32 [16384, 4], P('ep'), may hold values from 0.1 to 1
- norm_gain: float32 [2048], replicated, may hold values from 0.1 to 1.9
- gate_weight: bfloat16 [16, 2048, 1024], P('ep', None, 'tp'), may hold values from -0.125 to 0.125
- up_weight: bfloat16 [16, 2048, 1024], P('ep', None, 'tp'), may hold values from -0.125 to 0.125
- down_weight: bfloat16 [16, 1024, 2048], P('ep', 'tp'), may hold values from -0.1875 to 0.1875
- out_gain: float32 [2048], P('tp'), may hold values from 0.1 to 1.9
Outputs:
- mixed: bfloat16 [16384, 2048], P('ep', 'tp')
Inputs may be any that keep to these rules, and one draw needn't show every extreme that they name: `expert_ids`: each row names 4 different experts of 0 to 15; within the rows of one device (aligned blocks of 128 rows) no expert is named more than 64 times, and in some blocks one expert is named exactly 64 times.
All inputs are finite; a program needn't handle non-finite values.
Results may differ from a plain program's by a relative error of at most 0.0025.
Values may be sent and summed in bfloat16 or wider, within the bound.
No kernel may reach another device: no remote copies, remote signals or barrier semaphores. Data moves between devices by JAX's collectives and lax.ppermute only.
A program may use at most 64 MiB of HBM per device.

v0:
```python
import jax
import jax.numpy as jnp
from jax import lax
from jax.sharding import PartitionSpec as P

epsilon = 1e-05
clamp_limit = 7.0
sigmoid_alpha = 1.702


def taken_in(shard, axis, dim, absorb, state):
    everything = jax.tree.map(lambda a: lax.all_gather(a, axis, axis=dim, tiled=True), shard)
    return absorb(state, everything, jnp.int32(0))


def rms_rows(values, gain):
    mean_sq = jnp.mean(values * values, axis=-1, keepdims=True)
    return values * lax.rsqrt(mean_sq + epsilon) * gain


def clamped_unit(gate_part, up_part):
    glu_part = jnp.minimum(gate_part, clamp_limit)
    lin_part = jnp.clip(up_part, -clamp_limit, clamp_limit)
    return glu_part * jax.nn.sigmoid(sigmoid_alpha * glu_part) * (lin_part + 1.0)


def local(
    tokens, expert_ids, gate_values, norm_gain, gate_weight, up_weight, down_weight, out_gain
):
    expert_groups = lax.axis_size("ep")
    width_groups = lax.axis_size("tp")
    tok_rows = tokens.shape[0]
    model_width = tokens.shape[1]
    top_count = expert_ids.shape[1]
    capacity = tok_rows // 2
    per_rank = capacity // width_groups
    slice_w = model_width // width_groups
    normed = rms_rows(tokens.astype(jnp.float32), norm_gain).astype(jnp.bfloat16)
    blocks = expert_ids.reshape(width_groups, tok_rows * top_count)
    onehot = (
        blocks[:, :, None] == jnp.arange(expert_groups, dtype=jnp.int32)[None, None, :]
    ).astype(jnp.int32)
    slot_num = jnp.sum((jnp.cumsum(onehot, axis=1) - onehot) * onehot, axis=2)
    own_rank = lax.axis_index("tp")
    own_ids = lax.dynamic_index_in_dim(blocks, own_rank, 0, keepdims=False)
    own_slots = lax.dynamic_index_in_dim(slot_num, own_rank, 0, keepdims=False)
    target = own_ids * capacity + own_slots
    entry_token = jnp.arange(tok_rows * top_count, dtype=jnp.int32) // top_count
    owner_row = (
        jnp.full((expert_groups * capacity,), tok_rows, jnp.int32).at[target].set(entry_token)
    )
    padded = jnp.concatenate([normed, jnp.zeros((1, model_width), jnp.bfloat16)], axis=0)
    outgoing = padded[owner_row].reshape(expert_groups * width_groups, per_rank, model_width)
    arrived = lax.all_to_all(outgoing, ("ep", "tp"), split_axis=0, concat_axis=0, tiled=True)
    arrived_rows = arrived.reshape(-1, model_width)
    row_total = arrived_rows.shape[0]
    hidden_width = gate_weight.shape[2] * width_groups
    blank_acts = jnp.zeros((row_total, hidden_width), jnp.bfloat16)

    def add_hidden(activated, pieces, offset):
        gate_part = jnp.dot(arrived_rows, pieces[0][0], preferred_element_type=jnp.float32)
        up_part = jnp.dot(arrived_rows, pieces[1][0], preferred_element_type=jnp.float32)
        fresh = clamped_unit(gate_part, up_part).astype(jnp.bfloat16)
        return lax.dynamic_update_slice_in_dim(activated, fresh, offset, 1)

    activated = taken_in((gate_weight, up_weight), "tp", 2, add_hidden, blank_acts)

    def add_output(running, w_piece, offset):
        act_part = lax.dynamic_slice_in_dim(activated, offset, w_piece.shape[1], 1)
        return running + jnp.dot(act_part, w_piece[0], preferred_element_type=jnp.float32)

    blank_out = jnp.zeros((row_total, model_width), jnp.float32)
    result = taken_in(down_weight, "tp", 1, add_output, blank_out).astype(jnp.bfloat16)
    outbound = result.reshape(expert_groups, width_groups, per_rank, width_groups, slice_w)
    outbound = outbound.transpose(0, 3, 1, 2, 4)
    landed = lax.all_to_all(
        outbound.reshape(expert_groups * width_groups, width_groups, per_rank, slice_w),
        ("ep", "tp"),
        split_axis=0,
        concat_axis=0,
        tiled=True,
    )
    returned = landed.reshape(-1, slice_w)
    rank_part = slot_num // per_rank
    within = slot_num % per_rank
    source_col = jnp.arange(width_groups, dtype=jnp.int32)[:, None]
    row_index = (
        (blocks * width_groups + rank_part) * width_groups + source_col
    ) * per_rank + within
    picked = returned[row_index.reshape(-1)].astype(jnp.float32)
    picked = picked.reshape(width_groups * tok_rows, top_count, slice_w)
    combined = jnp.sum(gate_values[:, :, None] * picked, axis=1)
    local_sq = jnp.sum(combined * combined, axis=1)
    total_sq = lax.psum(local_sq, "tp")
    row_scale = lax.rsqrt(total_sq / model_width + epsilon)
    return (combined * row_scale[:, None] * out_gain).astype(jnp.bfloat16)


def solution(mesh):
    in_specs = (
        P(("ep", "tp"), None),
        P("ep", None),
        P("ep", None),
        P(),
        P("ep", None, "tp"),
        P("ep", None, "tp"),
        P("ep", "tp", None),
        P("tp"),
    )
    out_specs = P("ep", "tp")
    return jax.shard_map(local, mesh=mesh, in_specs=in_specs, out_specs=out_specs, check_vma=False)
```

profile of v0, /device:TPU:1, one launch (start us, length us, event | category | flops | bytes accessed | tf_op | source)
XLA Modules:
  0.0 281.1 jit_solution(7951599097116689879)
XLA Ops:
  6.5 0.0 copy-start
  6.5 0.0 copy-start.3
  6.5 0.0 all-gather.6.cloned.1.call-start
  6.5 0.7 all-gather.6.cloned.1.call-update
  7.3 0.0 all-gather.4.cloned.1.call-start
  7.3 0.7 all-gather.4.cloned.1.call-update
  8.0 0.0 all-gather.8.cloned.1.call-start
  8.1 0.7 all-gather.8.cloned.1.call-update
  8.7 0.9 copy.11
  9.7 0.3 eq.28
  10.0 0.3 reshape.220
  10.3 9.1 %reduce-window.6 = s32[8,16,4,128]{3,1,2,0:T(8,128)S(1)} reduce-window(s32[8,16,4,128]{3,1,2,0:T(8,128)S(1)} %fusion.21, s32[]{:T(128)} %constant.77.clone.1), window={size=1x1x1x128 pad=0_0x0_0x0_0x127_0}, to_apply=%region_1.0 | reduce-window | flops 8323072 | bytes 524292 | tf_op jit(solution)/shard_map/reduce-window
  19.4 0.1 slice.12
  19.5 0.3 copy.13
  19.8 0.1 fusion.23
  19.9 0.0 copy-done
  19.9 0.2 fusion.15
  20.1 0.0 copy-done.3
  20.1 0.2 fusion.17
  20.4 0.1 fusion.20
  20.6 2.4 scatter_custom_fusion
  23.0 6.0 %gather_fusion = bf16[1024,2048]{1,0:T(8,128)(2,1)} fusion(bf16[129,2048]{1,0:T(8,128)(2,1)S(1)} %concatenate.3, s32[1024]{0:T(1024)S(1)} %fusion.25), kind=kCustom, calls=%fused_computation | custom fusion | bytes 8392704 | tf_op jit(solution)/shard_map/gather | solution.py:53
  29.1 64.7 %all_to_all.10 = bf16[128,8,2048]{2,1,0:T(8,128)(2,1)} all-to-all(bf16[128,8,2048]{2,1,0:T(8,128)(2,1)} %bitcast.62), channel_id=1, replica_groups=mesh['ep'=16,'tp'=8] {'ep','tp'}, dimensions={0} | all-to-all | bytes 8388608 | tf_op jit(solution)/shard_map/all_to_all | solution.py:54
  93.7 0.0 all-gather.6.cloned.1.call-done
  93.7 9.9 %fusion.2 = f32[1024,1024]{1,0:T(8,128)} fusion(bf16[1,2048,1024]{2,1,0:T(8,128)(2,1)} %all-gather.6.cloned.1.call-done, bf16[128,8,2048]{2,1,0:T(8,128)(2,1)} %all_to_all.10), kind=kOutput, calls=%fused_computation.5 | convolution fusion | flops 4294967296 | bytes 12582912 | tf_op jit(solution)/shard_map/dot_general | solution.py:62
  103.6 26.1 %all-gather.4.cloned.1.call-done = bf16[1,2048,1024]{2,1,0:T(8,128)(2,1)} async-done(((bf16[1,2048,128]{2,1,0:T(8,128)(2,1)}), bf16[1,2048,1024]{2,1,0:T(8,128)(2,1)}) %all-gather.4.cloned.1.call-update) | async-done | bytes 4194320 | tf_op jit(solution)/shard_map/all_gather | solution.py:12
  129.7 10.1 %multiply_convert_fusion = bf16[1024,1024]{1,0:T(8,128)(2,1)S(1)} fusion(f32[1024,1024]{1,0:T(8,128)} %fusion.2, bf16[1,2048,1024]{2,1,0:T(8,128)(2,1)} %all-gather.4.cloned.1.call-done, bf16[128,8,2048]{2,1,0:T(8,128)(2,1)} %all_to_all.10), kind=kOutput, calls=%fused_computation.12 | convolution fusion | flops 4305453056 | bytes 14680064 | tf_op jit(solution)/shard_map/dot_general | solution.py:61
  139.8 24.7 %all-gather.8.cloned.1.call-done = bf16[1,1024,2048]{2,1,0:T(8,128)(2,1)} async-done(((bf16[1,128,2048]{2,1,0:T(8,128)(2,1)}), bf16[1,1024,2048]{2,1,0:T(8,128)(2,1)}) %all-gather.8.cloned.1.call-update) | async-done | bytes 4194320 | tf_op jit(solution)/shard_map/all_gather | solution.py:12
  164.5 6.9 %fusion.8 = bf16[1024,2048]{1,0:T(8,128)(2,1)S(1)} fusion(bf16[1024,1024]{1,0:T(8,128)(2,1)S(1)} %multiply_convert_fusion, bf16[1,1024,2048]{2,1,0:T(8,128)(2,1)} %all-gather.8.cloned.1.call-done), kind=kOutput, calls=%fused_computation.13 | convolution fusion | flops 4297064448 | bytes 10485760 | tf_op jit(solution)/shard_map/dot_general | solution.py:70
  171.3 2.6 copy.16
  173.9 0.0 copy-start.1
  173.9 0.0 copy-start.2
  173.9 8.3 %all-to-all-start.1 = ((bf16[128,8,8,256]{3,2,1,0:T(8,128)(2,1)}), bf16[128,8,8,256]{3,2,1,0:T(8,128)(2,1)}, u32[]{:S(2)}, u32[]{:S(2)}) async-start(bf16[128,8,8,256]{3,2,1,0:T(8,128)(2,1)} %bitcast.63), calls=%async_computation.1 | async-start | bytes 8388608 | tf_op jit(solution)/shard_map/all_to_all | solution.py:76
  182.2 0.0 copy-done.1
  182.3 0.2 copy.17
  182.5 0.3 mul.125
  182.9 0.0 copy-done.2
  182.9 0.2 copy.10
  183.1 0.2 compare_select_fusion
  183.3 51.6 %all-to-all-done.1 = bf16[128,8,8,256]{3,2,1,0:T(8,128)(2,1)} async-done(((bf16[128,8,8,256]{3,2,1,0:T(8,128)(2,1)}), bf16[128,8,8,256]{3,2,1,0:T(8,128)(2,1)}, u32[]{:S(2)}, u32[]{:S(2)}) %all-to-all-start.1) | async-done | bytes 4194336 | tf_op jit(solution)/shard_map/all_to_all | solution.py:76
  234.9 15.7 %gather_fusion.1 = bf16[4096,256]{1,0:T(8,128)(2,1)S(1)} fusion(bf16[8192,256]{1,0:T(8,128)(2,1)} %bitcast.12, s32[4096]{0:T(1024)S(1)} %broadcast_clamp_fusion), kind=kCustom, calls=%fused_computation.1 | custom fusion | bytes 4210688 | tf_op jit(solution)/shard_map/gather | solution.py:90
  250.6 2.9 %reshape.227 = f32[1024,4,256]{2,1,0:T(4,128)} reshape(bf16[4096,256]{1,0:T(8,128)(2,1)S(1)} %gather_fusion.1) | data formatting | bytes 6291456 | tf_op jit(solution)/shard_map/convert_element_type | solution.py:90
  253.5 0.0 copy-start.4
  253.5 7.2 %multiply_reduce_fusion = f32[1024,256]{1,0:T(8,128)S(1)} fusion(f32[1024,4,256]{2,1,0:T(4,128)} %reshape.227, f32[1024,4]{1,0:T(8,128)S(1)} %copy.10), kind=kLoop, calls=%fused_computation.11 | loop fusion | flops 1835008 | bytes 5259264 | tf_op jit(solution)/shard_map/reduce_sum | solution.py:92
  260.7 0.2 multiply_reduce_fusion.1
  260.9 12.7 %psum.7 = f32[1024]{0:T(1024)S(1)} all-reduce(f32[1024]{0:T(1024)S(1)} %multiply_reduce_fusion.1), channel_id=1, replica_groups=mesh['ep'=16,'tp'=8] {'tp'}, use_global_device_ids=true, to_apply=%region_7.8 | all-reduce | flops 1024 | bytes 8192 | tf_op jit(solution)/shard_map/psum | solution.py:94
  273.6 0.0 copy-done.4
  273.6 1.0 multiply_convert_fusion.1
  (14 shorter events, 0.2 us)
Async XLA Ops:
  6.5 13.4 %copy-start = (bf16[128,2048]{1,0:T(8,128)(2,1)S(1)}, bf16[128,2048]{1,0:T(8,128)(2,1)}, u32[]{:S(2)}) copy-start(bf16[128,2048]{1,0:T(8,128)(2,1)} %param.8) | copy-start | bytes 1572868
  6.5 13.6 %copy-start.3 = (f32[2048]{0:T(1024)S(1)}, f32[2048]{0:T(1024)}, u32[]{:S(2)}) copy-start(f32[2048]{0:T(1024)} %param.11) | copy-start | bytes 24580
  6.5 87.2 %all-gather.6.cloned.1.call-start = ((), (), s32[]{:S(2)}) async-start(), calls=%async_computation.3 | async-start | bytes 4718592 | tf_op jit(solution)/shard_map/all_gather | solution.py:12
  7.3 122.5 %all-gather.4.cloned.1.call-start = ((), (), s32[]{:S(2)}) async-start(), calls=%async_computation.2 | async-start | bytes 4718592 | tf_op jit(solution)/shard_map/all_gather | solution.py:12
  8.0 156.4 %all-gather.8.cloned.1.call-start = ((), (), s32[]{:S(2)}) async-start(), calls=%async_computation.4 | async-start | bytes 4718592 | tf_op jit(solution)/shard_map/all_gather | solution.py:12
  173.9 8.3 %copy-start.1 = (s32[1024,4]{0,1:T(4,128)S(1)}, s32[1024,4]{0,1:T(4,128)}, u32[]{:S(2)}) copy-start(s32[1024,4]{0,1:T(4,128)} %param.9) | copy-start | bytes 49156
  173.9 9.0 %copy-start.2 = (f32[1024,4]{0,1:T(4,128)S(1)}, f32[1024,4]{0,1:T(4,128)}, u32[]{:S(2)}) copy-start(f32[1024,4]{0,1:T(4,128)} %param.10) | copy-start | bytes 49156
  173.9 61.0 %all-to-all-start.1 = ((bf16[128,8,8,256]{3,2,1,0:T(8,128)(2,1)}), bf16[128,8,8,256]{3,2,1,0:T(8,128)(2,1)}, u32[]{:S(2)}, u32[]{:S(2)}) async-start(bf16[128,8,8,256]{3,2,1,0:T(8,128)(2,1)} %bitcast.63), calls=%async_computation.1 | async-start | bytes 8388608 | tf_op jit(solution)/shard_map/all_to_all | solution.py:76
  253.5 20.1 %copy-start.4 = (f32[256]{0:T(256)S(1)}, f32[256]{0:T(256)}, u32[]{:S(2)}) copy-start(f32[256]{0:T(256)} %param.15) | copy-start | bytes 3076
Sparse Core Ops, SparseCore 0:
  9.0 63.1 all-gather.5
  73.9 55.8 all-gather.3
  131.4 32.9 all-gather.7
where the time goes:
time: 282 us; the launch traced here: 281 us
  waiting for transfers between devices  105 us (37%)
  blocking collectives  77.4 us (27%)
  local copies, waits for them, and re-layouts  32.4 us (11%)
  matrix products  26.8 us (10%)
  other arithmetic  18.3 us (6%)
  between operations  13.4 us (5%)
  starting transfers between devices  8.37 us (3%)
    all_to_all x1, blocking collectives, local(): lax.all_to_all(outgoing, ('ep', 'tp'), split_axis=0, concat_axis=0, tiled...  64.7 us
    all_to_all x1, waiting for transfers between devices, local(): lax.all_to_all(outbound.reshape(expert_groups * width_groups, width_group...  51.6 us
    all_gather x3, waiting for transfers between devices, taken_in(): lax.all_gather(a, axis, axis=dim, tiled=True)  50.8 us
    gather x1, local copies, waits for them, and re-layouts, local(): picked = returned[row_index.reshape(-1)].astype(jnp.float32)  15.7 us
    psum x1, blocking collectives, local(): total_sq = lax.psum(local_sq, 'tp')  12.7 us
    dot_general x1, matrix products, add_hidden(): jnp.dot(arrived_rows, pieces[0][0], preferred_element_type=jnp.float32)  10.1 us
    dot_general x1, matrix products, add_hidden(): jnp.dot(arrived_rows, pieces[1][0], preferred_element_type=jnp.float32)  9.88 us
    another operation x2, other arithmetic  9.2 us
  transfers between devices with their start and end apart: 4, of which 3 were waited for; matrix products, arithmetic and copies ran while one was open for 15% of the time, Pallas kernels for 0%

commit v1 on v0

--- a/solution.py
+++ b/solution.py
@@ -1,3 +1,4 @@
+import functools
 import jax
 import jax.numpy as jnp
 from jax import lax
@@ -6,6 +7,24 @@
 epsilon = 1e-05
 clamp_limit = 7.0
 sigmoid_alpha = 1.702
+
+
+def assign_spot_now(point, lane_axis):
+    n_blocks = lax.psum(1, axis_name=lane_axis)
+
+    def expand_tails_over_axis(prior, field_out):
+        if field_out >= n_blocks:
+            return prior
+        return expand_tails_over_axis(
+            prior
+            + lax.ppermute(prior, lane_axis, perm=[(c, c ^ field_out) for c in range(n_blocks)]),
+            2 * field_out,
+        )
+
+    return expand_tails_over_axis(point, 1)
+
+
+produce_masks_here = functools.partial(assign_spot_now, lane_axis="tp")
 
 
 def taken_in(shard, axis, dim, absorb, state):
@@ -91,7 +110,7 @@
     picked = picked.reshape(width_groups * tok_rows, top_count, slice_w)
     combined = jnp.sum(gate_values[:, :, None] * picked, axis=1)
     local_sq = jnp.sum(combined * combined, axis=1)
-    total_sq = lax.psum(local_sq, "tp")
+    total_sq = produce_masks_here(local_sq)
     row_scale = lax.rsqrt(total_sq / model_width + epsilon)
     return (combined * row_scale[:, None] * out_gain).astype(jnp.bfloat16)
 

time: 282 us -> 278 us (0.986)
  blocking collectives: 77.4 us -> 64.7 us
  waiting for transfers between devices: 105 us -> 111 us
    psum x1 -> x0, blocking collectives: 12.7 us -> none  [local(): total_sq = lax.psum(local_sq, 'tp')]
    ppermute x0 -> x3, waiting for transfers between devices: none -> 6.95 us  [expand_tails_over_axis(): lax.ppermute(prior, lane_axis, perm=[(c, c ^ field_out) for c in range(n_...]
  transfers between devices with their start and end apart: 4 -> 7, of which waited for: 3 -> 6; matrix products, arithmetic and copies ran while one was open for 15% -> 15% of each run, Pallas kernels for 0% -> 0%
where the time goes in v1:
time: 278 us; the launch traced here: 277 us
  waiting for transfers between devices  111 us (40%)
  blocking collectives  64.7 us (23%)
  local copies, waits for them, and re-layouts  32.4 us (12%)
  matrix products  26.8 us (10%)
  other arithmetic  18.3 us (7%)
  between operations  13.4 us (5%)
  starting transfers between devices  9.67 us (3%)
    all_to_all x1, blocking collectives, local(): lax.all_to_all(outgoing, ('ep', 'tp'), split_axis=0, concat_axis=0, tiled...  64.7 us
    all_to_all x1, waiting for transfers between devices, local(): lax.all_to_all(outbound.reshape(expert_groups * width_groups, width_group...  51.6 us
    all_gather x3, waiting for transfers between devices, taken_in(): lax.all_gather(a, axis, axis=dim, tiled=True)  50.8 us
    gather x1, local copies, waits for them, and re-layouts, local(): picked = returned[row_index.reshape(-1)].astype(jnp.float32)  15.7 us
    dot_general x1, matrix products, add_hidden(): jnp.dot(arrived_rows, pieces[0][0], preferred_element_type=jnp.float32)  10.1 us
    dot_general x1, matrix products, add_hidden(): jnp.dot(arrived_rows, pieces[1][0], preferred_element_type=jnp.float32)  9.88 us
    another operation x2, other arithmetic  9.2 us
    all_to_all x1, starting transfers between devices, local(): lax.all_to_all(outbound.reshape(expert_groups * width_groups, width_group...  8.29 us
  transfers between devices with their start and end apart: 7, of which 6 were waited for; matrix products, arithmetic and copies ran while one was open for 15% of the time, Pallas kernels for 0%

profile of v1, /device:TPU:1, one launch (start us, length us, event | category | flops | bytes accessed | tf_op | source)
XLA Modules:
  0.0 276.7 jit_solution(16185036298853536639)
XLA Ops:
  6.5 0.0 copy-start
  6.5 0.0 copy-start.3
  6.5 0.0 all-gather.6.cloned.1.call-start
  6.5 0.7 all-gather.6.cloned.1.call-update
  7.3 0.0 all-gather.4.cloned.1.call-start
  7.3 0.7 all-gather.4.cloned.1.call-update
  8.0 0.0 all-gather.8.cloned.1.call-start
  8.1 0.7 all-gather.8.cloned.1.call-update
  8.7 0.9 copy.11
  9.7 0.3 eq.28
  10.0 0.3 reshape.220
  10.3 9.1 %reduce-window.6 = s32[8,16,4,128]{3,1,2,0:T(8,128)S(1)} reduce-window(s32[8,16,4,128]{3,1,2,0:T(8,128)S(1)} %fusion.21, s32[]{:T(128)} %constant.77.clone.1), window={size=1x1x1x128 pad=0_0x0_0x0_0x127_0}, to_apply=%region_1.0 | reduce-window | flops 8323072 | bytes 524292 | tf_op jit(solution)/shard_map/reduce-window
  19.4 0.1 slice.12
  19.5 0.3 copy.13
  19.8 0.1 fusion.23
  19.9 0.0 copy-done
  19.9 0.2 fusion.15
  20.1 0.0 copy-done.3
  20.1 0.2 fusion.17
  20.4 0.1 fusion.20
  20.6 2.4 scatter_custom_fusion
  23.0 6.0 %gather_fusion = bf16[1024,2048]{1,0:T(8,128)(2,1)} fusion(bf16[129,2048]{1,0:T(8,128)(2,1)S(1)} %concatenate.3, s32[1024]{0:T(1024)S(1)} %fusion.25), kind=kCustom, calls=%fused_computation | custom fusion | bytes 8392704 | tf_op jit(solution)/shard_map/gather | solution.py:72
  29.1 64.7 %all_to_all.10 = bf16[128,8,2048]{2,1,0:T(8,128)(2,1)} all-to-all(bf16[128,8,2048]{2,1,0:T(8,128)(2,1)} %bitcast.62), channel_id=1, replica_groups=mesh['ep'=16,'tp'=8] {'ep','tp'}, dimensions={0} | all-to-all | bytes 8388608 | tf_op jit(solution)/shard_map/all_to_all | solution.py:73
  93.7 0.0 all-gather.6.cloned.1.call-done
  93.7 9.9 %fusion.2 = f32[1024,1024]{1,0:T(8,128)} fusion(bf16[1,2048,1024]{2,1,0:T(8,128)(2,1)} %all-gather.6.cloned.1.call-done, bf16[128,8,2048]{2,1,0:T(8,128)(2,1)} %all_to_all.10), kind=kOutput, calls=%fused_computation.5 | convolution fusion | flops 4294967296 | bytes 12582912 | tf_op jit(solution)/shard_map/dot_general | solution.py:81
  103.6 26.1 %all-gather.4.cloned.1.call-done = bf16[1,2048,1024]{2,1,0:T(8,128)(2,1)} async-done(((bf16[1,2048,128]{2,1,0:T(8,128)(2,1)}), bf16[1,2048,1024]{2,1,0:T(8,128)(2,1)}) %all-gather.4.cloned.1.call-update) | async-done | bytes 4194320 | tf_op jit(solution)/shard_map/all_gather | solution.py:31
  129.7 10.1 %multiply_convert_fusion = bf16[1024,1024]{1,0:T(8,128)(2,1)S(1)} fusion(f32[1024,1024]{1,0:T(8,128)} %fusion.2, bf16[1,2048,1024]{2,1,0:T(8,128)(2,1)} %all-gather.4.cloned.1.call-done, bf16[128,8,2048]{2,1,0:T(8,128)(2,1)} %all_to_all.10), kind=kOutput, calls=%fused_computation.12 | convolution fusion | flops 4305453056 | bytes 14680064 | tf_op jit(solution)/shard_map/dot_general | solution.py:80
  139.8 24.7 %all-gather.8.cloned.1.call-done = bf16[1,1024,2048]{2,1,0:T(8,128)(2,1)} async-done(((bf16[1,128,2048]{2,1,0:T(8,128)(2,1)}), bf16[1,1024,2048]{2,1,0:T(8,128)(2,1)}) %all-gather.8.cloned.1.call-update) | async-done | bytes 4194320 | tf_op jit(solution)/shard_map/all_gather | solution.py:31
  164.5 6.9 %fusion.8 = bf16[1024,2048]{1,0:T(8,128)(2,1)S(1)} fusion(bf16[1024,1024]{1,0:T(8,128)(2,1)S(1)} %multiply_convert_fusion, bf16[1,1024,2048]{2,1,0:T(8,128)(2,1)} %all-gather.8.cloned.1.call-done), kind=kOutput, calls=%fused_computation.13 | convolution fusion | flops 4297064448 | bytes 10485760 | tf_op jit(solution)/shard_map/dot_general | solution.py:89
  171.3 2.6 copy.16
  173.9 0.0 copy-start.1
  173.9 0.0 copy-start.2
  173.9 8.3 %all-to-all-start.1 = ((bf16[128,8,8,256]{3,2,1,0:T(8,128)(2,1)}), bf16[128,8,8,256]{3,2,1,0:T(8,128)(2,1)}, u32[]{:S(2)}, u32[]{:S(2)}) async-start(bf16[128,8,8,256]{3,2,1,0:T(8,128)(2,1)} %bitcast.63), calls=%async_computation.1 | async-start | bytes 8388608 | tf_op jit(solution)/shard_map/all_to_all | solution.py:95
  182.2 0.0 copy-done.1
  182.3 0.2 copy.17
  182.5 0.3 mul.125
  182.9 0.0 copy-done.2
  182.9 0.2 copy.10
  183.1 0.2 compare_select_fusion
  183.3 51.6 %all-to-all-done.1 = bf16[128,8,8,256]{3,2,1,0:T(8,128)(2,1)} async-done(((bf16[128,8,8,256]{3,2,1,0:T(8,128)(2,1)}), bf16[128,8,8,256]{3,2,1,0:T(8,128)(2,1)}, u32[]{:S(2)}, u32[]{:S(2)}) %all-to-all-start.1) | async-done | bytes 4194336 | tf_op jit(solution)/shard_map/all_to_all | solution.py:95
  234.9 15.7 %gather_fusion.1 = bf16[4096,256]{1,0:T(8,128)(2,1)S(1)} fusion(bf16[8192,256]{1,0:T(8,128)(2,1)} %bitcast.12, s32[4096]{0:T(1024)S(1)} %broadcast_clamp_fusion), kind=kCustom, calls=%fused_computation.1 | custom fusion | bytes 4210688 | tf_op jit(solution)/shard_map/gather | solution.py:109
  250.6 2.9 %reshape.227 = f32[1024,4,256]{2,1,0:T(4,128)} reshape(bf16[4096,256]{1,0:T(8,128)(2,1)S(1)} %gather_fusion.1) | data formatting | bytes 6291456 | tf_op jit(solution)/shard_map/convert_element_type | solution.py:109
  253.5 0.0 copy-start.4
  253.5 7.2 %multiply_reduce_fusion = f32[1024,256]{1,0:T(8,128)S(1)} fusion(f32[1024,4,256]{2,1,0:T(4,128)} %reshape.227, f32[1024,4]{1,0:T(8,128)S(1)} %copy.10), kind=kLoop, calls=%fused_computation.11 | loop fusion | flops 1835008 | bytes 5259264 | tf_op jit(solution)/shard_map/reduce_sum | solution.py:111
  260.7 0.2 multiply_reduce_fusion.1
  260.9 1.0 collective-permute-start
  261.9 0.8 collective-permute-done
  262.7 0.2 collective-permute-start.1
  262.9 2.3 collective-permute-done.1
  265.2 0.1 collective-permute-start.2
  265.3 3.9 %collective-permute-done.2 = f32[1024]{0:T(1024)S(1)} collective-permute-done((f32[1024]{0:T(1024)S(1)}, f32[1024]{0:T(1024)S(1)}, u32[]{:S(2)}, u32[]{:S(2)}) %collective-permute-start.2) | collective-permute-done | bytes 4128 | tf_op jit(solution)/shard_map/ppermute | solution.py:20
  269.2 0.0 copy-done.4
  269.2 1.0 multiply_convert_fusion.1
  (16 shorter events, 0.2 us)
Async XLA Ops:
  6.5 13.4 %copy-start = (bf16[128,2048]{1,0:T(8,128)(2,1)S(1)}, bf16[128,2048]{1,0:T(8,128)(2,1)}, u32[]{:S(2)}) copy-start(bf16[128,2048]{1,0:T(8,128)(2,1)} %param.8) | copy-start | bytes 1572868
  6.5 13.6 %copy-start.3 = (f32[2048]{0:T(1024)S(1)}, f32[2048]{0:T(1024)}, u32[]{:S(2)}) copy-start(f32[2048]{0:T(1024)} %param.11) | copy-start | bytes 24580
  6.5 87.2 %all-gather.6.cloned.1.call-start = ((), (), s32[]{:S(2)}) async-start(), calls=%async_computation.3 | async-start | bytes 4718592 | tf_op jit(solution)/shard_map/all_gather | solution.py:31
  7.3 122.5 %all-gather.4.cloned.1.call-start = ((), (), s32[]{:S(2)}) async-start(), calls=%async_computation.2 | async-start | bytes 4718592 | tf_op jit(solution)/shard_map/all_gather | solution.py:31
  8.0 156.4 %all-gather.8.cloned.1.call-start = ((), (), s32[]{:S(2)}) async-start(), calls=%async_computation.4 | async-start | bytes 4718592 | tf_op jit(solution)/shard_map/all_gather | solution.py:31
  173.9 8.3 %copy-start.1 = (s32[1024,4]{0,1:T(4,128)S(1)}, s32[1024,4]{0,1:T(4,128)}, u32[]{:S(2)}) copy-start(s32[1024,4]{0,1:T(4,128)} %param.9) | copy-start | bytes 49156
  173.9 9.0 %copy-start.2 = (f32[1024,4]{0,1:T(4,128)S(1)}, f32[1024,4]{0,1:T(4,128)}, u32[]{:S(2)}) copy-start(f32[1024,4]{0,1:T(4,128)} %param.10) | copy-start | bytes 49156
  173.9 61.0 %all-to-all-start.1 = ((bf16[128,8,8,256]{3,2,1,0:T(8,128)(2,1)}), bf16[128,8,8,256]{3,2,1,0:T(8,128)(2,1)}, u32[]{:S(2)}, u32[]{:S(2)}) async-start(bf16[128,8,8,256]{3,2,1,0:T(8,128)(2,1)} %bitcast.63), calls=%async_computation.1 | async-start | bytes 8388608 | tf_op jit(solution)/shard_map/all_to_all | solution.py:95
  253.5 15.7 %copy-start.4 = (f32[256]{0:T(256)S(1)}, f32[256]{0:T(256)}, u32[]{:S(2)}) copy-start(f32[256]{0:T(256)} %param.15) | copy-start | bytes 3076
  260.9 1.8 collective-permute-start
  262.7 2.5 collective-permute-start.1
  265.2 4.0 %collective-permute-start.2 = (f32[1024]{0:T(1024)S(1)}, f32[1024]{0:T(1024)S(1)}, u32[]{:S(2)}, u32[]{:S(2)}) collective-permute-start(f32[1024]{0:T(1024)S(1)} %add.168), channel_id=1, source_target_pairs={{0,4},{1,5},{2,6},{3,7},{4,0},{5,1},{6,2},{7,3},{8,12},{9,13},{10,... | collective-permute-start | bytes 12296 | tf_op jit(solution)/shard_map/ppermute | solution.py:20
Sparse Core Ops, SparseCore 0:
  9.0 63.1 all-gather.5
  73.9 55.8 all-gather.3
  131.4 32.9 all-gather.7
